TPU v7x, 32 devices: a whole 2x2x4 slice. The times are simulated.
32 devices in a mesh: sp: 8 (over z, y), tp: 4 (over x, core).
Axes of the slice: x: 2, y: 2, z: 4, core: 2. Of those that a mesh axis runs over, the one named last changes fastest.
Arguments:
- tokens: bfloat16 [2048, 2048], P('sp', 'tp'), may hold values from -6 to 6
- in_gain: float32 [2048], replicated, may hold values from 0.1 to 1.9
- query_down: bfloat16 [2048, 512], replicated, may hold values from -0.125 to 0.125
- latent_down: bfloat16 [2048, 256], replicated, may hold values from -0.125 to 0.125
- rope_down: bfloat16 [2048, 32], replicated, may hold values from -0.125 to 0.125
- query_gain: float32 [512], replicated, may hold values from 0.5 to 12
- latent_gain: float32 [256], replicated, may hold values from 0.5 to 12
- query_nope: bfloat16 [512, 1024], P(None, 'tp'), may hold values from -0.25 to 0.25
- query_rope: bfloat16 [512, 512], P(None, 'tp'), may hold values from -0.25 to 0.25
- key_up: bfloat16 [256, 1024], P(None, 'tp'), may hold values from -0.375 to 0.375
- value_up: bfloat16 [256, 1024], P(None, 'tp'), may hold values from -0.375 to 0.375
- conv_value: bfloat16 [2048, 2048], P(None, 'tp'), may hold values from -0.125 to 0.125
- conv_gate: bfloat16 [2048, 2048], P(None, 'tp'), may hold values from -0.125 to 0.125
- conv_taps: float32 [31, 2048], P(None, 'tp'), may hold values from -1 to 1
- conv_bias: float32 [2048], P('tp'), may hold values from 0.05 to 2.25
- channel_gain: float32 [2048], P('tp'), may hold values from 0.1 to 1.9
- out_attend: bfloat16 [1024, 2048], P('tp'), may hold values from -0.109375 to 0.109375
- out_conv: bfloat16 [2048, 2048], P('tp'), may hold values from -0.109375 to 0.109375
Outputs:
- mixed: bfloat16 [2048, 2048], P('sp', 'tp')
All inputs are finite; a program needn't handle non-finite values.
Results may differ from a plain program's by a relative error of at most 0.013.
The roundings to bfloat16 on the way count: a program that leaves them out, or rounds other values in their place, can miss the bound.
Values may be sent and summed in bfloat16 or wider, within the bound.
A program may use at most 128 MiB of HBM per device.

v0:
```python
import math
import jax
import jax.numpy as jnp
from jax import lax
from jax.sharding import PartitionSpec as P

eps_norm = 1e-06
eps_layer = 1e-05
theta = 10000.0


def padded_2(cells, sides, width):
    for axis, dim in sides:
        count = lax.axis_size(axis)
        ends = count - 1
        head = lax.slice_in_dim(cells, 0, width, axis=dim)
        tail = lax.slice_in_dim(cells, cells.shape[dim] - width, cells.shape[dim], axis=dim)
        cells = jnp.concatenate(
            [
                lax.ppermute(tail, axis, [(i, (i + 1) % count) for i in range(ends)]),
                cells,
                lax.ppermute(head, axis, [((i + 1) % count, i) for i in range(ends)]),
            ],
            axis=dim,
        )
    return cells


def rms_scale(values, gain):
    return values * lax.rsqrt(jnp.mean(values * values, axis=-1, keepdims=True) + eps_norm) * gain


def rotate(values, positions):
    half = values.shape[-1] // 2
    freqs = theta ** (-jnp.arange(half).astype(jnp.float32) / half)
    angles = positions[..., None] * freqs
    cosine = jnp.cos(angles)
    sine = jnp.sin(angles)
    first = values[..., :half]
    second = values[..., half:]
    return jnp.concatenate(
        [first * cosine - second * sine, second * cosine + first * sine], axis=-1
    )


def attend_block(state, q_heads, r_heads, k_nope, values, rope_key):
    highest, total, weighted = state
    heads = q_heads.shape[1]
    key_heads = k_nope.reshape(k_nope.shape[0], heads, -1)
    value_heads = values.reshape(values.shape[0], heads, -1)
    score_scale = (q_heads.shape[2] + r_heads.shape[2]) ** (-0.5)
    scores = (
        jnp.einsum("qhd,khd->hqk", q_heads, key_heads, preferred_element_type=jnp.float32)
        + jnp.einsum("qhd,kd->hqk", r_heads, rope_key, preferred_element_type=jnp.float32)
    ) * score_scale
    new_high = jnp.maximum(highest, jnp.max(scores, axis=-1))
    factor = jnp.exp(highest - new_high)
    weight = jnp.exp(scores - new_high[..., None])
    total = total * factor + jnp.sum(weight, axis=-1)
    weighted = weighted * factor[..., None] + jnp.einsum(
        "hqk,khd->hqd", weight.astype(jnp.bfloat16), value_heads, preferred_element_type=jnp.float32
    )
    return (new_high, total, weighted)


def over_blocks(state, arrays, step):
    count = arrays[0].shape[0]
    size = math.gcd(count, 1024)
    shaped = tuple((item.reshape((count // size, size) + item.shape[1:]) for item in arrays))

    def one_block(carry, block):
        return (step(carry, block), None)

    state, unused = lax.scan(one_block, state, shaped)
    return state


def per_device(
    tokens,
    in_gain,
    query_down,
    latent_down,
    rope_down,
    query_gain,
    latent_gain,
    query_nope,
    query_rope,
    key_up,
    value_up,
    conv_value,
    conv_gate,
    conv_taps,
    conv_bias,
    channel_gain,
    out_attend,
    out_conv,
):
    row_count = tokens.shape[0]
    width = in_gain.shape[0]
    local_ch = conv_value.shape[1]
    positions = (lax.axis_index("sp") * row_count + jnp.arange(row_count)).astype(jnp.float32)
    piece_f = lax.all_gather(tokens, "tp", axis=1, tiled=True).astype(jnp.float32)
    scaled = (piece_f * in_gain).astype(jnp.bfloat16)

    def add_rows(weight):
        return jnp.dot(scaled, weight, preferred_element_type=jnp.float32)

    square_sum = jnp.sum(piece_f * piece_f, axis=1)
    q_pre = add_rows(query_down)
    kv_pre = add_rows(latent_down)
    rope_pre = add_rows(rope_down)
    value_pre = add_rows(conv_value)
    gate_pre = add_rows(conv_gate)
    row_scale = lax.rsqrt(square_sum / width + eps_norm)[:, None]
    q_latent = rms_scale(row_scale * q_pre, query_gain).astype(jnp.bfloat16)
    kv_latent = rms_scale(row_scale * kv_pre, latent_gain).astype(jnp.bfloat16)
    rope_key = rotate(row_scale * rope_pre, positions).astype(jnp.bfloat16)
    rope_size = rope_down.shape[1]
    heads = query_rope.shape[1] // rope_size
    q_heads = (
        jnp.dot(q_latent, query_nope, preferred_element_type=jnp.float32)
        .astype(jnp.bfloat16)
        .reshape(row_count, heads, -1)
    )
    q_turn = jnp.dot(q_latent, query_rope, preferred_element_type=jnp.float32).reshape(
        row_count, heads, rope_size
    )
    r_heads = rotate(q_turn, positions[:, None]).astype(jnp.bfloat16)
    value_size = value_up.shape[1] // heads
    start_state = (
        jnp.full((heads, row_count), -jnp.inf, jnp.float32),
        jnp.zeros((heads, row_count), jnp.float32),
        jnp.zeros((heads, row_count, value_size), jnp.float32),
    )

    def latent_step(state, block):
        k_nope = jnp.dot(block[0], key_up, preferred_element_type=jnp.float32).astype(jnp.bfloat16)
        values = jnp.dot(block[0], value_up, preferred_element_type=jnp.float32).astype(
            jnp.bfloat16
        )
        return attend_block(state, q_heads, r_heads, k_nope, values, block[1])

    highest, total, weighted = over_blocks(
        start_state,
        (
            lax.all_gather(kv_latent, "sp", axis=0, tiled=True),
            lax.all_gather(rope_key, "sp", axis=0, tiled=True),
        ),
        latent_step,
    )
    attended = jnp.transpose((weighted / total[..., None]).astype(jnp.bfloat16), (1, 0, 2)).reshape(
        row_count, heads * value_size
    )
    glu = (row_scale * value_pre * jax.nn.sigmoid(row_scale * gate_pre)).astype(jnp.bfloat16)
    taps = conv_taps.shape[0]
    padded = padded_2(glu, (("sp", 0),), taps // 2).astype(jnp.float32)
    conv = jnp.zeros((row_count, local_ch), jnp.float32) + conv_bias
    for tap in range(taps):
        conv = conv + conv_taps[tap] * padded[tap : tap + row_count]
    channels = local_ch * lax.axis_size("tp")
    first_sum, second_sum = lax.psum((jnp.sum(conv, axis=-1), jnp.sum(conv * conv, axis=-1)), "tp")
    mean = first_sum[:, None] / channels
    spread = second_sum[:, None] / channels - mean * mean
    centred = conv - mean
    activated = jax.nn.silu(centred * lax.rsqrt(spread + eps_layer) * channel_gain).astype(
        jnp.bfloat16
    )
    contract = (((0,), (1,)), ((), ()))
    summed = lax.psum_scatter(
        (
            lax.dot_general(out_attend, attended, contract, preferred_element_type=jnp.float32)
            + lax.dot_general(out_conv, activated, contract, preferred_element_type=jnp.float32)
        ).astype(jnp.bfloat16),
        "tp",
        scatter_dimension=0,
        tiled=True,
    ).astype(jnp.float32)
    return jnp.transpose(summed).astype(jnp.bfloat16)


def solution(mesh):
    in_specs = (
        P("sp", "tp"),
        P(),
        P(),
        P(),
        P(),
        P(),
        P(),
        P(None, "tp"),
        P(None, "tp"),
        P(None, "tp"),
        P(None, "tp"),
        P(None, "tp"),
        P(None, "tp"),
        P(None, "tp"),
        P("tp"),
        P("tp"),
        P("tp", None),
        P("tp", None),
    )
    out_specs = P("sp", "tp")
    return jax.shard_map(
        per_device, mesh=mesh, in_specs=in_specs, out_specs=out_specs, check_vma=False
    )
```

profile of v0, /device:TPU:0, one launch (start us, length us, event | category | flops | bytes accessed | tf_op | source)
XLA Modules:
  0.0 147.2 jit_solution(18445132968032190985)
XLA Ops:
  8.5 1.6 %fusion.76 = (f32[1,512]{1,0:T(1,128)}, f32[1,512]{1,0:T(1,128)}, f32[1,512]{1,0:T(1,128)}, f32[1,512]{1,0:T(1,128)}, f32[1,512]{1,0:T(1,128)}, /*index=5*/f32[1...) fusion(f32[31,512]{1,0:T(8,128)} %param.33), kind=kLoop, calls=%fused_computation.139 | loop fusion | bytes 49152 | tf_op jit(solution)/shard_map/slice | solution.py:159
  10.1 1.8 %fusion.75 = (f32[1,512]{1,0:T(1,128)}, f32[1,512]{1,0:T(1,128)}, f32[1,512]{1,0:T(1,128)}, f32[1,512]{1,0:T(1,128)}, f32[1,512]{1,0:T(1,128)}, /*index=5*/f32[1...) fusion(f32[31,512]{1,0:T(8,128)} %param.33), kind=kLoop, calls=%fused_computation.138 | loop fusion | bytes 77824 | tf_op jit(solution)/shard_map/slice | solution.py:159
  12.0 16.4 %all-gather.3.cloned.1.call-done = bf16[256,2048]{1,0:T(8,128)(2,1)} async-done(((bf16[256,512]{1,0:T(8,128)(2,1)}), bf16[256,2048]{1,0:T(8,128)(2,1)}) %all-gather.3.cloned.1.call-update) | async-done | bytes 1048592 | tf_op jit(solution)/shard_map/all_gather | solution.py:102
  28.3 1.5 %fusion.21 = f32[256]{0:T(256)S(1)} fusion(bf16[256,2048]{1,0:T(8,128)(2,1)} %all-gather.3.cloned.1.call-done), kind=kLoop, calls=%fused_computation.29 | loop fusion | flops 1572608 | bytes 1049600 | tf_op jit(solution)/shard_map/reduce_sum | solution.py:108
  29.9 2.9 %fusion.26 = f32[256,512]{1,0:T(8,128)S(1)} fusion(bf16[2048,512]{1,0:T(8,128)(2,1)} %param.32, bf16[256,2048]{1,0:T(8,128)(2,1)} %all-gather.3.cloned.1.call-done, f32[2048]{0:T(1024)} %param.21, f32[256]{0:T(256)S(1)} %add_rsqrt_fusion.3), kind=kOutput, calls=%fused_computation.35 | convolution fusion | flops 538968064 | bytes 3679232 | tf_op jit(solution)/shard_map/dot_general | solution.py:106
  34.2 4.0 %collective-permute-start = (bf16[15,512]{1,0:T(8,128)(2,1)}, bf16[15,512]{1,0:T(8,128)(2,1)}, u32[]{:S(2)}, u32[]{:S(2)}) collective-permute-start(bf16[15,512]{1,0:T(8,128)(2,1)} %get-tuple-element.132), channel_id=1, source_target_pairs={{0,4},{4,8},{8,12},{12,16},{16,20},{20,24},{24,28},{1,5},{5,9},{9,... | collective-permute-start | bytes 46088 | tf_op jit(solution)/shard_map/ppermute | solution.py:20
  38.1 1.4 collective-permute-start.1
  39.6 0.8 multiply_reduce_fusion.1
  41.9 1.7 %convolution_multiply_fusion.4 = f32[256,32]{0,1:T(8,128)S(1)} fusion(bf16[2048,32]{0,1:T(8,128)(2,1)} %param.24, bf16[256,2048]{1,0:T(8,128)(2,1)} %all-gather.3.cloned.1.call-done, f32[2048]{0:T(1024)} %param.21, f32[256]{0:T(256)} %copy-done.41), kind=kOutput, calls=%fused_computation.42 | convolution fusion | flops 35135488 | bytes 1221632 | tf_op jit(solution)/shard_map/dot_general | solution.py:106
  43.9 0.8 multiply_cosine_fusion
  45.7 1.3 convolution_convert_fusion.2
  47.0 32.4 %all_gather.11 = bf16[2048,32]{0,1:T(8,128)(2,1)S(1)} all-gather(bf16[256,32]{0,1:T(8,128)(2,1)S(1)} %pad_maximum_fusion.1), channel_id=1, replica_groups=mesh['sp'=8,'tp'=4] {'sp'}, dimensions={0}, use_global_device_ids=true | all-gather | bytes 147456 | tf_op jit(solution)/shard_map/all_gather | solution.py:147
  80.1 0.8 maximum_convert_fusion
  81.2 3.3 %fusion.71 = (f32[256]{0:T(256)S(1)}, f32[256]{0:T(256)S(1)}, f32[256,512]{1,0:T(8,128)}) fusion(f32[286,512]{1,0:T(8,128)S(1)} %maximum_convert_fusion, f32[512]{0:T(512)S(1)} %bitcast.119, f32[512]{0:T(512)S(1)} %bitcast.120, f32[512]{0:T(512)S(1)} %bitcast.122, f32[512]{0:T(512)S(1)} %bitcast.123, f32[512]{0:T(512)S(1)} %bitcast.124, ...), kind=kLoop, calls=%fused_computation.135 | loop fusion | flops 8519168 | bytes 16844800 | tf_op jit(solution)/shard_map/reduce_sum | solution.py:161
  84.5 5.6 %all-reduce = (f32[256]{0:T(256)S(1)}, f32[256]{0:T(256)S(1)}) all-reduce(f32[256]{0:T(256)S(1)} %get-tuple-element.104, f32[256]{0:T(256)S(1)} %get-tuple-element.103), channel_id=1, replica_groups=mesh['sp'=8,'tp'=4] {'tp'}, use_global_device_ids=true, to_apply=%region_10.11 | all-reduce | flops 512 | bytes 4096 | tf_op jit(solution)/shard_map/psum | solution.py:161
  90.7 1.5 %copy.23 = bf16[2048,256]{1,0:T(8,128)(2,1)S(1)} copy(bf16[2048,256]{0,1:T(8,128)(2,1)} %all-gather.5.cloned.1.call-done) | data formatting | bytes 2097152
  92.2 19.9 %while.15 = (s32[]{:T(128)}, f32[4,256]{1,0:T(4,128)S(1)}, f32[4,256]{1,0:T(4,128)S(1)}, f32[4,256,64]{1,2,0:T(8,128)S(1)}, bf16[2,1024,256]{2,1,0:T(8,128)(2,1)...) while((s32[]{:T(128)}, f32[4,256]{1,0:T(4,128)S(1)}, ...), condition=%wide.region_6.7_spmd.clone, body=%wide.region_3.6_spmd.clone.sunk | while | flops 612045824 | bytes 42795232 | solution.py:74
  92.2 1.2 convolution_convert_fusion.5
  93.5 0.8 fusion.118
  94.4 2.7 %fusion.119 = (f32[4,256]{1,0:T(4,128)S(1)}, f32[4,256,1024]{1,2,0:T(8,128)}) fusion(bf16[256,4,32]{0,2,1:T(8,128)(2,1)S(1)} %copy-done.2, bf16[2,1024,32]{1,2,0:T(8,128)(2,1)S(1)} %copy-done.3, s32[]{:T(128)} %get-tuple-element.260, f32[4,1024,256]{2,1,0:T(8,128)S(1)} %fusion.118), kind=kOutput, calls=%fused_computation.136.clone.1 | convolution fusion | flops 70253568 | bytes 8523780 | tf_op jit(solution)/shard_map/while/body/eval_jaxpr/qhd,kd->hqk/dot_general | solution.py:54
  97.1 2.9 %fusion.120 = f32[4,256]{1,0:T(4,128)S(1)} fusion(f32[4,256,1024]{1,2,0:T(8,128)} %get-tuple-element.245, f32[4,256]{1,0:T(4,128)S(1)} %select_maximum_fusion.2), kind=kLoop, calls=%fused_computation.4.clone.1 | loop fusion | flops 2096128 | bytes 4202496 | tf_op jit(solution)/shard_map/while/body/eval_jaxpr/reduce_sum | solution.py:59
  100.0 1.3 convolution_convert_fusion.6
  101.3 0.8 fusion.122
  102.1 1.2 convolution_convert_fusion.5
  103.4 0.8 fusion.118
  104.3 2.7 %fusion.119 = (f32[4,256]{1,0:T(4,128)S(1)}, f32[4,256,1024]{1,2,0:T(8,128)}) fusion(bf16[256,4,32]{0,2,1:T(8,128)(2,1)S(1)} %copy-done.2, bf16[2,1024,32]{1,2,0:T(8,128)(2,1)S(1)} %copy-done.3, s32[]{:T(128)} %get-tuple-element.260, f32[4,1024,256]{2,1,0:T(8,128)S(1)} %fusion.118), kind=kOutput, calls=%fused_computation.136.clone.1 | convolution fusion | flops 70253568 | bytes 8523780 | tf_op jit(solution)/shard_map/while/body/eval_jaxpr/qhd,kd->hqk/dot_general | solution.py:54
  107.1 2.9 %fusion.120 = f32[4,256]{1,0:T(4,128)S(1)} fusion(f32[4,256,1024]{1,2,0:T(8,128)} %get-tuple-element.245, f32[4,256]{1,0:T(4,128)S(1)} %select_maximum_fusion.2), kind=kLoop, calls=%fused_computation.4.clone.1 | loop fusion | flops 2096128 | bytes 4202496 | tf_op jit(solution)/shard_map/while/body/eval_jaxpr/reduce_sum | solution.py:59
  110.0 1.2 convolution_convert_fusion.6
  111.3 0.8 fusion.122
  112.2 1.7 %fusion.78 = f32[256,2048]{1,0:T(8,128)S(1)} fusion(bf16[256,256]{0,1:T(8,128)(2,1)S(1)} %bitcast.106, bf16[256,2048]{1,0:T(8,128)(2,1)} %param.36), kind=kOutput, calls=%fused_computation.141 | convolution fusion | flops 268435456 | bytes 3276800 | tf_op jit(solution)/shard_map/dot_general | solution.py:171
  113.9 1.9 %fusion.20 = bf16[2048,256]{0,1:T(8,128)(2,1)} fusion(f32[256,2048]{1,0:T(8,128)S(1)} %fusion.78, bf16[512,2048]{1,0:T(8,128)(2,1)S(1)} %copy-done, f32[256,512]{1,0:T(8,128)S(1)} %copy-done.5, f32[512]{0:T(512)S(1)} %copy-done.47, f32[256]{0:T(256)S(1)} %copy-done.42, f32[256]{0:T(256)S(1)} %get-tuple-element.173), kind=kOutput, calls=%fused_computation.28 | convolution fusion | flops 538968064 | bytes 5771264 | tf_op jit(solution)/shard_map/dot_general | solution.py:172
  115.8 24.9 %reduce-scatter.2.cloned.1.call-done = bf16[512,256]{0,1:T(8,128)(2,1)} async-done(((bf16[2048,256]{0,1:T(8,128)(2,1)}), bf16[512,256]{0,1:T(8,128)(2,1)}) %reduce-scatter.2.cloned.1.call-update) | async-done | bytes 262160 | tf_op jit(solution)/shard_map/reduce_scatter | solution.py:169
  (136 shorter events, 7.6 us)
Async XLA Ops:
  6.5 107.4 %copy-start = (bf16[512,2048]{1,0:T(8,128)(2,1)S(1)}, bf16[512,2048]{1,0:T(8,128)(2,1)}, u32[]{:S(2)}) copy-start(bf16[512,2048]{1,0:T(8,128)(2,1)} %param.37) | copy-start | bytes 6291460
  6.5 21.8 %all-gather.3.cloned.1.call-start = ((), (), s32[]{:S(2)}) async-start(), calls=%async_computation.1 | async-start | bytes 1310720 | tf_op jit(solution)/shard_map/all_gather | solution.py:102
  7.3 83.4 %all-gather.5.cloned.1.call-start = ((), (), s32[]{:S(2)}) async-start(), calls=%async_computation.2 | async-start | bytes 1179648 | tf_op jit(solution)/shard_map/all_gather | solution.py:146
  34.2 45.9 %collective-permute-start = (bf16[15,512]{1,0:T(8,128)(2,1)}, bf16[15,512]{1,0:T(8,128)(2,1)}, u32[]{:S(2)}, u32[]{:S(2)}) collective-permute-start(bf16[15,512]{1,0:T(8,128)(2,1)} %get-tuple-element.132), channel_id=1, source_target_pairs={{0,4},{4,8},{8,12},{12,16},{16,20},{20,24},{24,28},{1,5},{5,9},{9,... | collective-permute-start | bytes 46088 | tf_op jit(solution)/shard_map/ppermute | solution.py:20
  38.1 41.9 %collective-permute-start.1 = (bf16[15,512]{1,0:T(8,128)(2,1)}, bf16[15,512]{1,0:T(8,128)(2,1)}, u32[]{:S(2)}, u32[]{:S(2)}) collective-permute-start(bf16[15,512]{1,0:T(8,128)(2,1)} %get-tuple-element.133), channel_id=1, source_target_pairs={{4,0},{8,4},{12,8},{16,12},{20,16},{24,20},{28,24},{5,1},{9,5},{13... | collective-permute-start | bytes 46088 | tf_op jit(solution)/shard_map/ppermute | solution.py:22
  41.8 98.9 %reduce-scatter.2.cloned.1.call-start = ((), (), s32[]{:S(2)}) async-start(), calls=%async_computation.3 | async-start | bytes 1310720 | tf_op jit(solution)/shard_map/reduce_scatter | solution.py:169
  43.6 37.3 %copy-start.8 = (f32[1,512]{1,0:T(1,128)S(1)}, f32[1,512]{1,0:T(1,128)}, u32[]{:S(2)}) copy-start(f32[1,512]{1,0:T(1,128)} %get-tuple-element.155) | copy-start | bytes 6148
  43.6 37.3 %copy-start.9 = (f32[1,512]{1,0:T(1,128)S(1)}, f32[1,512]{1,0:T(1,128)}, u32[]{:S(2)}) copy-start(f32[1,512]{1,0:T(1,128)} %get-tuple-element.156) | copy-start | bytes 6148
  43.6 37.3 %copy-start.10 = (f32[1,512]{1,0:T(1,128)S(1)}, f32[1,512]{1,0:T(1,128)}, u32[]{:S(2)}) copy-start(f32[1,512]{1,0:T(1,128)} %get-tuple-element.157) | copy-start | bytes 6148
  43.6 37.3 %copy-start.11 = (f32[1,512]{1,0:T(1,128)S(1)}, f32[1,512]{1,0:T(1,128)}, u32[]{:S(2)}) copy-start(f32[1,512]{1,0:T(1,128)} %get-tuple-element.158) | copy-start | bytes 6148
  43.6 37.3 %copy-start.12 = (f32[1,512]{1,0:T(1,128)S(1)}, f32[1,512]{1,0:T(1,128)}, u32[]{:S(2)}) copy-start(f32[1,512]{1,0:T(1,128)} %get-tuple-element.159) | copy-start | bytes 6148
  43.6 37.3 %copy-start.13 = (f32[1,512]{1,0:T(1,128)S(1)}, f32[1,512]{1,0:T(1,128)}, u32[]{:S(2)}) copy-start(f32[1,512]{1,0:T(1,128)} %get-tuple-element.160) | copy-start | bytes 6148
  43.6 37.3 %copy-start.14 = (f32[1,512]{1,0:T(1,128)S(1)}, f32[1,512]{1,0:T(1,128)}, u32[]{:S(2)}) copy-start(f32[1,512]{1,0:T(1,128)} %get-tuple-element.161) | copy-start | bytes 6148
  43.6 37.3 %copy-start.15 = (f32[1,512]{1,0:T(1,128)S(1)}, f32[1,512]{1,0:T(1,128)}, u32[]{:S(2)}) copy-start(f32[1,512]{1,0:T(1,128)} %get-tuple-element.162) | copy-start | bytes 6148
  43.6 37.3 %copy-start.16 = (f32[1,512]{1,0:T(1,128)S(1)}, f32[1,512]{1,0:T(1,128)}, u32[]{:S(2)}) copy-start(f32[1,512]{1,0:T(1,128)} %get-tuple-element.163) | copy-start | bytes 6148
  43.6 37.3 %copy-start.17 = (f32[1,512]{1,0:T(1,128)S(1)}, f32[1,512]{1,0:T(1,128)}, u32[]{:S(2)}) copy-start(f32[1,512]{1,0:T(1,128)} %get-tuple-element.164) | copy-start | bytes 6148
  43.7 37.3 %copy-start.18 = (f32[1,512]{1,0:T(1,128)S(1)}, f32[1,512]{1,0:T(1,128)}, u32[]{:S(2)}) copy-start(f32[1,512]{1,0:T(1,128)} %get-tuple-element.165) | copy-start | bytes 6148
  43.7 37.3 %copy-start.19 = (f32[1,512]{1,0:T(1,128)S(1)}, f32[1,512]{1,0:T(1,128)}, u32[]{:S(2)}) copy-start(f32[1,512]{1,0:T(1,128)} %get-tuple-element.166) | copy-start | bytes 6148
  43.7 37.3 %copy-start.20 = (f32[1,512]{1,0:T(1,128)S(1)}, f32[1,512]{1,0:T(1,128)}, u32[]{:S(2)}) copy-start(f32[1,512]{1,0:T(1,128)} %get-tuple-element.136) | copy-start | bytes 6148
  43.7 37.3 %copy-start.21 = (f32[1,512]{1,0:T(1,128)S(1)}, f32[1,512]{1,0:T(1,128)}, u32[]{:S(2)}) copy-start(f32[1,512]{1,0:T(1,128)} %get-tuple-element.137) | copy-start | bytes 6148
  43.7 37.3 %copy-start.22 = (f32[1,512]{1,0:T(1,128)S(1)}, f32[1,512]{1,0:T(1,128)}, u32[]{:S(2)}) copy-start(f32[1,512]{1,0:T(1,128)} %get-tuple-element.138) | copy-start | bytes 6148
  43.7 37.3 %copy-start.23 = (f32[1,512]{1,0:T(1,128)S(1)}, f32[1,512]{1,0:T(1,128)}, u32[]{:S(2)}) copy-start(f32[1,512]{1,0:T(1,128)} %get-tuple-element.139) | copy-start | bytes 6148
  43.7 37.3 %copy-start.24 = (f32[1,512]{1,0:T(1,128)S(1)}, f32[1,512]{1,0:T(1,128)}, u32[]{:S(2)}) copy-start(f32[1,512]{1,0:T(1,128)} %get-tuple-element.140) | copy-start | bytes 6148
  43.7 37.3 %copy-start.25 = (f32[1,512]{1,0:T(1,128)S(1)}, f32[1,512]{1,0:T(1,128)}, u32[]{:S(2)}) copy-start(f32[1,512]{1,0:T(1,128)} %get-tuple-element.141) | copy-start | bytes 6148
  43.7 37.3 %copy-start.26 = (f32[1,512]{1,0:T(1,128)S(1)}, f32[1,512]{1,0:T(1,128)}, u32[]{:S(2)}) copy-start(f32[1,512]{1,0:T(1,128)} %get-tuple-element.142) | copy-start | bytes 6148
  43.7 37.3 %copy-start.27 = (f32[1,512]{1,0:T(1,128)S(1)}, f32[1,512]{1,0:T(1,128)}, u32[]{:S(2)}) copy-start(f32[1,512]{1,0:T(1,128)} %get-tuple-element.143) | copy-start | bytes 6148
  43.8 37.3 %copy-start.28 = (f32[1,512]{1,0:T(1,128)S(1)}, f32[1,512]{1,0:T(1,128)}, u32[]{:S(2)}) copy-start(f32[1,512]{1,0:T(1,128)} %get-tuple-element.144) | copy-start | bytes 6148
  43.8 37.3 %copy-start.29 = (f32[1,512]{1,0:T(1,128)S(1)}, f32[1,512]{1,0:T(1,128)}, u32[]{:S(2)}) copy-start(f32[1,512]{1,0:T(1,128)} %get-tuple-element.145) | copy-start | bytes 6148
  43.8 37.3 %copy-start.30 = (f32[1,512]{1,0:T(1,128)S(1)}, f32[1,512]{1,0:T(1,128)}, u32[]{:S(2)}) copy-start(f32[1,512]{1,0:T(1,128)} %get-tuple-element.146) | copy-start | bytes 6148
  43.8 37.3 %copy-start.31 = (f32[1,512]{1,0:T(1,128)S(1)}, f32[1,512]{1,0:T(1,128)}, u32[]{:S(2)}) copy-start(f32[1,512]{1,0:T(1,128)} %get-tuple-element.147) | copy-start | bytes 6148
  43.8 37.3 %copy-start.32 = (f32[1,512]{1,0:T(1,128)S(1)}, f32[1,512]{1,0:T(1,128)}, u32[]{:S(2)}) copy-start(f32[1,512]{1,0:T(1,128)} %get-tuple-element.148) | copy-start | bytes 6148
  43.8 37.3 %copy-start.33 = (f32[1,512]{1,0:T(1,128)S(1)}, f32[1,512]{1,0:T(1,128)}, u32[]{:S(2)}) copy-start(f32[1,512]{1,0:T(1,128)} %get-tuple-element.149) | copy-start | bytes 6148
  (24 other events, 278.8 us)
Sparse Core Ops, SparseCore 0:
  8.9 19.4 all-gather.2
  42.0 40.8 all-gather.4
  116.0 24.6 reduce-scatter.1
where the time goes:
time: 148 us; the launch traced here: 147 us
  waiting for transfers between devices  42 us (28%)
  blocking collectives  38 us (26%)
  matrix products  25.4 us (17%)
  other arithmetic  15.5 us (10%)
  between operations  13.9 us (9%)
  local copies, waits for them, and re-layouts  6.72 us (5%)
  starting transfers between devices  5.47 us (4%)
    all_gather x1, blocking collectives, per_device(): lax.all_gather(rope_key, 'sp', axis=0, tiled=True)  32.4 us
    reduce_scatter x1, waiting for transfers between devices, per_device(): lax.psum_scatter((lax.dot_general(out_attend, attended, contract, preferr...  24.9 us
    all_gather x1, waiting for transfers between devices, per_device(): lax.all_gather(tokens, 'tp', axis=1, tiled=True).astype(jnp.float32)  16.4 us
    dot_general x5, matrix products, add_rows(): return jnp.dot(scaled, weight, preferred_element_type=jnp.float32)  6.63 us
    reduce_sum x2, other arithmetic, attend_block(): total = total * factor + jnp.sum(weight, axis=-1)  5.81 us
    psum x1, blocking collectives, per_device(): lax.psum((jnp.sum(conv, axis=-1), jnp.sum(conv * conv, axis=-1)), 'tp')  5.63 us
    dot_general x2, matrix products, attend_block(): jnp.einsum('qhd,kd->hqk', r_heads, rope_key, preferred_element_type=jnp.f...  5.41 us
    ppermute x1, starting transfers between devices, padded_2(): lax.ppermute(tail, axis, [(i, (i + 1) % count) for i in range(ends)])  3.98 us
  transfers between devices with their start and end apart: 5, of which 2 were waited for; matrix products, arithmetic and copies ran while one was open for 11% of the time, Pallas kernels for 0%

commit v1 on v0

--- a/solution.py
+++ b/solution.py
@@ -1,12 +1,31 @@
+import functools
 import math
 import jax
 import jax.numpy as jnp
 from jax import lax
 from jax.sharding import PartitionSpec as P
+from jax.lax import axis_index, axis_size, ppermute
 
 eps_norm = 1e-06
 eps_layer = 1e-05
 theta = 10000.0
+
+
+def use_rails_now(a0, at_axis, shard_axis):
+    shares = axis_size(shard_axis)
+    views = [(dev, (dev + 1) % shares) for dev in range(shares)]
+    nodes = [(dev, (dev - 1) % shares) for dev in range(shares)]
+    v1, y_new = ([a0], [a0])
+    for _ in range(shares // 2):
+        v1.append(ppermute(v1[-1], shard_axis, views))
+    for _ in range((shares - 1) // 2):
+        y_new.append(ppermute(y_new[-1], shard_axis, nodes))
+    latest = jnp.concatenate([*v1[::-1], *y_new[1:]], at_axis)
+    mat_out = jnp.roll(latest, (axis_index(shard_axis) - shares // 2) * a0.shape[at_axis], at_axis)
+    return mat_out
+
+
+_serve_rails = functools.partial(use_rails_now, at_axis=1, shard_axis="tp")
 
 
 def padded_2(cells, sides, width):
@@ -99,7 +118,7 @@
     width = in_gain.shape[0]
     local_ch = conv_value.shape[1]
     positions = (lax.axis_index("sp") * row_count + jnp.arange(row_count)).astype(jnp.float32)
-    piece_f = lax.all_gather(tokens, "tp", axis=1, tiled=True).astype(jnp.float32)
+    piece_f = _serve_rails(tokens).astype(jnp.float32)
     scaled = (piece_f * in_gain).astype(jnp.bfloat16)
 
     def add_rows(weight):

time: 148 us -> 141 us (0.953)
  waiting for transfers between devices: 42 us -> 29.4 us
  starting transfers between devices: 5.47 us -> 12 us
  matrix products: 25.4 us -> 22.9 us
  local copies, waits for them, and re-layouts: 6.72 us -> 8.68 us
    all_gather x1 -> x0, waiting for transfers between devices: 16.4 us -> none  [per_device(): lax.all_gather(tokens, 'tp', axis=1, tiled=True).astype(jnp.float32)]
    ppermute x0 -> x3, starting transfers between devices: none -> 4.98 us  [the longest x2 3 us: use_rails_now(): v1.append(ppermute(v1[-1], shard_axis, views))]
    dot_general x5, matrix products: 6.63 us -> 3.3 us  [add_rows(): return jnp.dot(scaled, weight, preferred_element_type=jnp.float32)]
    ppermute x0 -> x3, waiting for transfers between devices: none -> 3.17 us  [the longest x2 3.17 us: use_rails_now(): v1.append(ppermute(v1[-1], shard_axis, views))]
    unnamed x91 -> x38, local copies, waits for them, and re-layouts: 1.69 us -> 3.63 us
    ppermute x1, starting transfers between devices: 3.98 us -> 5.58 us  [padded_2(): lax.ppermute(tail, axis, [(i, (i + 1) % count) for i in range(ends)])]
  transfers between devices with their start and end apart: 5 -> 7, of which waited for: 2 -> 3; matrix products, arithmetic and copies ran while one was open for 11% -> 13% of each run, Pallas kernels for 0% -> 0%
where the time goes in v1:
time: 141 us; the launch traced here: 140 us
  blocking collectives  38.6 us (27%)
  waiting for transfers between devices  29.4 us (21%)
  matrix products  22.9 us (16%)
  other arithmetic  14.6 us (10%)
  between operations  13.8 us (10%)
  starting transfers between devices  12 us (9%)
  local copies, waits for them, and re-layouts  8.68 us (6%)
    all_gather x1, blocking collectives, per_device(): lax.all_gather(rope_key, 'sp', axis=0, tiled=True)  32.9 us
    reduce_scatter x1, waiting for transfers between devices, per_device(): lax.psum_scatter((lax.dot_general(out_attend, attended, contract, preferr...  26.2 us
    reduce_sum x2, other arithmetic, attend_block(): total = total * factor + jnp.sum(weight, axis=-1)  5.81 us
    psum x1, blocking collectives, per_device(): lax.psum((jnp.sum(conv, axis=-1), jnp.sum(conv * conv, axis=-1)), 'tp')  5.76 us
    ppermute x1, starting transfers between devices, padded_2(): lax.ppermute(tail, axis, [(i, (i + 1) % count) for i in range(ends)])  5.58 us
    dot_general x2, matrix products, attend_block(): jnp.einsum('qhd,kd->hqk', r_heads, rope_key, preferred_element_type=jnp.f...  5.38 us
    reduce_sum x1, other arithmetic, per_device(): jnp.sum(conv, axis=-1)  4.27 us
    unnamed x38, local copies, waits for them, and re-layouts  3.63 us
  transfers between devices with their start and end apart: 7, of which 3 were waited for; matrix products, arithmetic and copies ran while one was open for 13% of the time, Pallas kernels for 0%

profile of v1, /device:TPU:0, one launch (start us, length us, event | category | flops | bytes accessed | tf_op | source)
XLA Modules:
  0.0 140.1 jit_solution(2870156354783790453)
XLA Ops:
  7.0 2.0 %collective-permute-start.2 = (bf16[256,512]{1,0:T(8,128)(2,1)}, bf16[256,512]{1,0:T(8,128)(2,1)S(1)}, u32[]{:S(2)}, u32[]{:S(2)}) collective-permute-start(bf16[256,512]{1,0:T(8,128)(2,1)} %param.20), channel_id=1, source_target_pairs={{0,3},{1,0},{2,1},{3,2},{4,7},{5,4},{6,5},{7,6},{8,11},{9,8},{10,9... | collective-permute-start | bytes 786440 | tf_op jit(solution)/shard_map/ppermute | solution.py:22
  9.6 1.6 %fusion.81 = (f32[1,512]{1,0:T(1,128)}, f32[1,512]{1,0:T(1,128)}, f32[1,512]{1,0:T(1,128)}, f32[1,512]{1,0:T(1,128)}, f32[1,512]{1,0:T(1,128)}, /*index=5*/f32[1...) fusion(f32[31,512]{1,0:T(8,128)} %param.33), kind=kLoop, calls=%fused_computation.152 | loop fusion | bytes 49152 | tf_op jit(solution)/shard_map/slice | solution.py:178
  11.2 2.3 %collective-permute-done = bf16[256,512]{1,0:T(8,128)(2,1)S(1)} collective-permute-done((bf16[256,512]{1,0:T(8,128)(2,1)}, bf16[256,512]{1,0:T(8,128)(2,1)S(1)}, u32[]{:S(2)}, u32[]{:S(2)}) %collective-permute-start) | collective-permute-done | bytes 262176 | tf_op jit(solution)/shard_map/ppermute | solution.py:20
  13.5 2.5 %collective-permute-start.1 = (bf16[256,512]{1,0:T(8,128)(2,1)S(1)}, bf16[256,512]{1,0:T(8,128)(2,1)S(1)}, u32[]{:S(2)}, u32[]{:S(2)}) collective-permute-start(bf16[256,512]{1,0:T(8,128)(2,1)S(1)} %collective-permute-done), channel_id=1, source_target_pairs={{0,1},{1,2},{2,3},{3,0},{4,5},{5,6},{6,7},{7,4},{8,9},{9,10},{10,1... | collective-permute-start | bytes 786440 | tf_op jit(solution)/shard_map/ppermute | solution.py:20
  16.6 1.8 %fusion.80 = (f32[1,512]{1,0:T(1,128)}, f32[1,512]{1,0:T(1,128)}, f32[1,512]{1,0:T(1,128)}, f32[1,512]{1,0:T(1,128)}, f32[1,512]{1,0:T(1,128)}, /*index=5*/f32[1...) fusion(f32[31,512]{1,0:T(8,128)} %param.33), kind=kLoop, calls=%fused_computation.151 | loop fusion | bytes 77824 | tf_op jit(solution)/shard_map/slice | solution.py:178
  18.4 0.9 collective-permute-done.1
  19.4 1.1 constant_dynamic-update-slice_fusion.5
  21.8 0.8 copy-done.12
  23.9 5.6 %collective-permute-start.3 = (bf16[15,512]{1,0:T(8,128)(2,1)}, bf16[15,512]{1,0:T(8,128)(2,1)}, u32[]{:S(2)}, u32[]{:S(2)}) collective-permute-start(bf16[15,512]{1,0:T(8,128)(2,1)} %get-tuple-element.132), channel_id=1, source_target_pairs={{0,4},{4,8},{8,12},{12,16},{16,20},{20,24},{24,28},{1,5},{5,9},{9,... | collective-permute-start | bytes 46088 | tf_op jit(solution)/shard_map/ppermute | solution.py:39
  29.5 1.4 %collective-permute-start.4 = (bf16[15,512]{1,0:T(8,128)(2,1)}, bf16[15,512]{1,0:T(8,128)(2,1)}, u32[]{:S(2)}, u32[]{:S(2)}) collective-permute-start(bf16[15,512]{1,0:T(8,128)(2,1)} %get-tuple-element.133), channel_id=1, source_target_pairs={{4,0},{8,4},{12,8},{16,12},{20,16},{24,20},{28,24},{5,1},{9,5},{13... | collective-permute-start | bytes 46088 | tf_op jit(solution)/shard_map/ppermute | solution.py:41
  30.9 0.8 multiply_reduce_fusion.1
  33.9 1.2 fusion.75
  35.7 1.3 convolution_convert_fusion.2
  37.0 32.9 %all_gather.7 = bf16[2048,32]{0,1:T(8,128)(2,1)S(1)} all-gather(bf16[256,32]{0,1:T(8,128)(2,1)S(1)} %pad_maximum_fusion.1), channel_id=1, replica_groups=mesh['sp'=8,'tp'=4] {'sp'}, dimensions={0}, use_global_device_ids=true | all-gather | bytes 147456 | tf_op jit(solution)/shard_map/all_gather | solution.py:166
  70.6 0.8 maximum_convert_fusion
  71.4 4.3 %fusion.76 = (f32[256]{0:T(256)S(1)}, f32[256]{0:T(256)S(1)}, f32[256,512]{1,0:T(8,128)}) fusion(f32[286,512]{1,0:T(8,128)S(1)} %maximum_convert_fusion, f32[512]{0:T(512)} %bitcast.119, f32[512]{0:T(512)} %bitcast.120, f32[512]{0:T(512)} %bitcast.122, f32[512]{0:T(512)} %bitcast.123, f32[512]{0:T(512)} %bitcast.124, f32[512]{0:T(512)} %bitcast.125, ...), kind=kLoop, calls=%fused_computation.148 | loop fusion | flops 8519168 | bytes 16844800 | tf_op jit(solution)/shard_map/reduce_sum | solution.py:180
  75.7 5.8 %all-reduce = (f32[256]{0:T(256)S(1)}, f32[256]{0:T(256)S(1)}) all-reduce(f32[256]{0:T(256)S(1)} %get-tuple-element.104, f32[256]{0:T(256)S(1)} %get-tuple-element.103), channel_id=1, replica_groups=mesh['sp'=8,'tp'=4] {'tp'}, use_global_device_ids=true, to_apply=%region_10.11 | all-reduce | flops 512 | bytes 4096 | tf_op jit(solution)/shard_map/psum | solution.py:180
  82.0 1.5 %copy.23 = bf16[2048,256]{1,0:T(8,128)(2,1)S(1)} copy(bf16[2048,256]{0,1:T(8,128)(2,1)} %all-gather.2.cloned.1.call-done) | data formatting | bytes 2097152
  83.5 19.9 %while.15 = (s32[]{:T(128)}, f32[4,256]{1,0:T(4,128)S(1)}, f32[4,256]{1,0:T(4,128)S(1)}, f32[4,256,64]{1,2,0:T(8,128)S(1)}, bf16[2,1024,256]{2,1,0:T(8,128)(2,1)...) while((s32[]{:T(128)}, f32[4,256]{1,0:T(4,128)S(1)}, ...), condition=%wide.region_6.7_spmd.clone, body=%wide.region_3.6_spmd.clone.sunk | while | flops 612045824 | bytes 42795232 | solution.py:93
  83.5 1.2 convolution_convert_fusion.5
  85.7 2.7 %fusion.124 = (f32[4,256]{1,0:T(4,128)S(1)}, f32[4,256,1024]{1,2,0:T(8,128)}) fusion(bf16[256,4,32]{0,2,1:T(8,128)(2,1)S(1)} %copy-done.2, bf16[2,1024,32]{1,2,0:T(8,128)(2,1)S(1)} %copy-done.3, s32[]{:T(128)} %get-tuple-element.260, f32[4,1024,256]{2,1,0:T(8,128)S(1)} %fusion.123), kind=kOutput, calls=%fused_computation.149.clone.1 | convolution fusion | flops 70253568 | bytes 8523780 | tf_op jit(solution)/shard_map/while/body/eval_jaxpr/qhd,kd->hqk/dot_general | solution.py:73
  88.4 2.9 %fusion.125 = f32[4,256]{1,0:T(4,128)S(1)} fusion(f32[4,256,1024]{1,2,0:T(8,128)} %get-tuple-element.245, f32[4,256]{1,0:T(4,128)S(1)} %select_maximum_fusion.2), kind=kLoop, calls=%fused_computation.4.clone.1 | loop fusion | flops 2096128 | bytes 4202496 | tf_op jit(solution)/shard_map/while/body/eval_jaxpr/reduce_sum | solution.py:78
  91.3 1.3 convolution_convert_fusion.6
  92.6 0.8 fusion.127
  93.4 1.2 convolution_convert_fusion.5
  95.6 2.7 %fusion.124 = (f32[4,256]{1,0:T(4,128)S(1)}, f32[4,256,1024]{1,2,0:T(8,128)}) fusion(bf16[256,4,32]{0,2,1:T(8,128)(2,1)S(1)} %copy-done.2, bf16[2,1024,32]{1,2,0:T(8,128)(2,1)S(1)} %copy-done.3, s32[]{:T(128)} %get-tuple-element.260, f32[4,1024,256]{2,1,0:T(8,128)S(1)} %fusion.123), kind=kOutput, calls=%fused_computation.149.clone.1 | convolution fusion | flops 70253568 | bytes 8523780 | tf_op jit(solution)/shard_map/while/body/eval_jaxpr/qhd,kd->hqk/dot_general | solution.py:73
  98.3 2.9 %fusion.125 = f32[4,256]{1,0:T(4,128)S(1)} fusion(f32[4,256,1024]{1,2,0:T(8,128)} %get-tuple-element.245, f32[4,256]{1,0:T(4,128)S(1)} %select_maximum_fusion.2), kind=kLoop, calls=%fused_computation.4.clone.1 | loop fusion | flops 2096128 | bytes 4202496 | tf_op jit(solution)/shard_map/while/body/eval_jaxpr/reduce_sum | solution.py:78
  101.2 1.3 convolution_convert_fusion.6
  102.5 0.8 fusion.127
  103.4 1.7 %fusion.83 = f32[256,2048]{1,0:T(8,128)S(1)} fusion(bf16[256,256]{0,1:T(8,128)(2,1)S(1)} %bitcast.106, bf16[256,2048]{1,0:T(8,128)(2,1)} %param.36), kind=kOutput, calls=%fused_computation.154 | convolution fusion | flops 268435456 | bytes 3276800 | tf_op jit(solution)/shard_map/dot_general | solution.py:190
  105.2 1.9 %fusion.20 = bf16[2048,256]{0,1:T(8,128)(2,1)} fusion(f32[256,2048]{1,0:T(8,128)S(1)} %fusion.83, bf16[512,2048]{1,0:T(8,128)(2,1)S(1)} %copy-done, f32[256,512]{1,0:T(8,128)S(1)} %copy-done.5, f32[512]{0:T(512)S(1)} %copy-done.17, f32[256]{0:T(256)S(1)} %copy-done.8, f32[256]{0:T(256)S(1)} %get-tuple-element.173), kind=kOutput, calls=%fused_computation.28 | convolution fusion | flops 538968064 | bytes 5771264 | tf_op jit(solution)/shard_map/dot_general | solution.py:191
  107.1 26.2 %reduce-scatter.2.cloned.1.call-done = bf16[512,256]{0,1:T(8,128)(2,1)} async-done(((bf16[2048,256]{0,1:T(8,128)(2,1)}), bf16[512,256]{0,1:T(8,128)(2,1)}) %reduce-scatter.2.cloned.1.call-update) | async-done | bytes 262160 | tf_op jit(solution)/shard_map/reduce_scatter | solution.py:188
  (87 shorter events, 10.1 us)
Async XLA Ops:
  6.5 98.6 %copy-start = (bf16[512,2048]{1,0:T(8,128)(2,1)S(1)}, bf16[512,2048]{1,0:T(8,128)(2,1)}, u32[]{:S(2)}) copy-start(bf16[512,2048]{1,0:T(8,128)(2,1)} %param.37) | copy-start | bytes 6291460
  6.5 14.1 %copy-start.4 = (bf16[256,512]{1,0:T(8,128)(2,1)S(1)}, bf16[256,512]{1,0:T(8,128)(2,1)}, u32[]{:S(2)}) copy-start(bf16[256,512]{1,0:T(8,128)(2,1)} %param.20) | copy-start | bytes 786436
  6.5 75.5 %all-gather.2.cloned.1.call-start = ((), (), s32[]{:S(2)}) async-start(), calls=%async_computation.1 | async-start | bytes 1179648 | tf_op jit(solution)/shard_map/all_gather | solution.py:165
  6.5 6.9 %collective-permute-start = (bf16[256,512]{1,0:T(8,128)(2,1)}, bf16[256,512]{1,0:T(8,128)(2,1)S(1)}, u32[]{:S(2)}, u32[]{:S(2)}) collective-permute-start(bf16[256,512]{1,0:T(8,128)(2,1)} %param.20), channel_id=1, source_target_pairs={{0,1},{1,2},{2,3},{3,0},{4,5},{5,6},{6,7},{7,4},{8,9},{9,10},{10,1... | collective-permute-start | bytes 786440 | tf_op jit(solution)/shard_map/ppermute | solution.py:20
  7.0 13.5 %collective-permute-start.2 = (bf16[256,512]{1,0:T(8,128)(2,1)}, bf16[256,512]{1,0:T(8,128)(2,1)S(1)}, u32[]{:S(2)}, u32[]{:S(2)}) collective-permute-start(bf16[256,512]{1,0:T(8,128)(2,1)} %param.20), channel_id=1, source_target_pairs={{0,3},{1,0},{2,1},{3,2},{4,7},{5,4},{6,5},{7,6},{8,11},{9,8},{10,9... | collective-permute-start | bytes 786440 | tf_op jit(solution)/shard_map/ppermute | solution.py:22
  13.5 5.8 %collective-permute-start.1 = (bf16[256,512]{1,0:T(8,128)(2,1)S(1)}, bf16[256,512]{1,0:T(8,128)(2,1)S(1)}, u32[]{:S(2)}, u32[]{:S(2)}) collective-permute-start(bf16[256,512]{1,0:T(8,128)(2,1)S(1)} %collective-permute-done), channel_id=1, source_target_pairs={{0,1},{1,2},{2,3},{3,0},{4,5},{5,6},{6,7},{7,4},{8,9},{9,10},{10,1... | collective-permute-start | bytes 786440 | tf_op jit(solution)/shard_map/ppermute | solution.py:20
  19.3 1.7 %copy-start.11 = (bf16[2048,512]{1,0:T(8,128)(2,1)S(1)}, bf16[2048,512]{1,0:T(8,128)(2,1)}, u32[]{:S(2)}) copy-start(bf16[2048,512]{1,0:T(8,128)(2,1)} %param.32) | copy-start | bytes 6291460
  19.4 1.7 %copy-start.16 = (f32[2048]{0:T(1024)S(1)}, f32[2048]{0:T(1024)}, u32[]{:S(2)}) copy-start(f32[2048]{0:T(1024)} %param.21) | copy-start | bytes 24580
  21.0 1.6 %copy-start.12 = (bf16[2048,512]{1,0:T(8,128)(2,1)S(1)}, bf16[2048,512]{1,0:T(8,128)(2,1)}, u32[]{:S(2)}) copy-start(bf16[2048,512]{1,0:T(8,128)(2,1)} %param.31) | copy-start | bytes 6291460
  22.6 8.3 %copy-start.13 = (bf16[2048,512]{1,0:T(8,128)(2,1)S(1)}, bf16[2048,512]{1,0:T(8,128)(2,1)}, u32[]{:S(2)}) copy-start(bf16[2048,512]{1,0:T(8,128)(2,1)} %param.22) | copy-start | bytes 6291460
  23.9 46.6 %collective-permute-start.3 = (bf16[15,512]{1,0:T(8,128)(2,1)}, bf16[15,512]{1,0:T(8,128)(2,1)}, u32[]{:S(2)}, u32[]{:S(2)}) collective-permute-start(bf16[15,512]{1,0:T(8,128)(2,1)} %get-tuple-element.132), channel_id=1, source_target_pairs={{0,4},{4,8},{8,12},{12,16},{16,20},{20,24},{24,28},{1,5},{5,9},{9,... | collective-permute-start | bytes 46088 | tf_op jit(solution)/shard_map/ppermute | solution.py:39
  29.5 2.2 %copy-start.15 = (bf16[2048,32]{0,1:T(8,128)(2,1)S(1)}, bf16[2048,32]{0,1:T(8,128)(2,1)}, u32[]{:S(2)}) copy-start(bf16[2048,32]{0,1:T(8,128)(2,1)} %param.24) | copy-start | bytes 393220
  29.5 2.7 %copy-start.14 = (bf16[2048,256]{1,0:T(8,128)(2,1)S(1)}, bf16[2048,256]{1,0:T(8,128)(2,1)}, u32[]{:S(2)}) copy-start(bf16[2048,256]{1,0:T(8,128)(2,1)} %param.23) | copy-start | bytes 3145732
  29.5 41.1 %collective-permute-start.4 = (bf16[15,512]{1,0:T(8,128)(2,1)}, bf16[15,512]{1,0:T(8,128)(2,1)}, u32[]{:S(2)}, u32[]{:S(2)}) collective-permute-start(bf16[15,512]{1,0:T(8,128)(2,1)} %get-tuple-element.133), channel_id=1, source_target_pairs={{4,0},{8,4},{12,8},{16,12},{20,16},{24,20},{28,24},{5,1},{9,5},{13... | collective-permute-start | bytes 46088 | tf_op jit(solution)/shard_map/ppermute | solution.py:41
  31.7 1.1 copy-start.7
  31.8 1.9 %copy-start.9 = (f32[256]{0:T(256)S(1)}, f32[256]{0:T(256)}, u32[]{:S(2)}) copy-start(f32[256]{0:T(256)} %add_convert_fusion.2) | copy-start | bytes 3076
  31.8 1.9 %copy-start.10 = (f32[16]{0:T(128)S(1)}, f32[16]{0:T(128)}, u32[]{:S(2)}) copy-start(f32[16]{0:T(128)} %multiply_power_fusion) | copy-start | bytes 196
  31.8 2.1 %copy-start.6 = (f32[512]{0:T(512)S(1)}, f32[512]{0:T(512)}, u32[]{:S(2)}) copy-start(f32[512]{0:T(512)} %param.25) | copy-start | bytes 6148
  33.6 99.6 %reduce-scatter.2.cloned.1.call-start = ((), (), s32[]{:S(2)}) async-start(), calls=%async_computation.2 | async-start | bytes 1310720 | tf_op jit(solution)/shard_map/reduce_scatter | solution.py:188
  84.7 0.8 copy-start.2
  84.8 0.9 copy-start.3
  88.4 4.2 %copy-start.1 = (f32[4,256,1024]{1,2,0:T(8,128)S(1)}, f32[4,256,1024]{1,2,0:T(8,128)}, u32[]{:S(2)}) copy-start(f32[4,256,1024]{1,2,0:T(8,128)} %get-tuple-element.245) | copy-start | bytes 12582916 | tf_op jit(solution)/shard_map/while
  94.7 0.8 copy-start.2
  94.7 0.9 copy-start.3
  98.3 4.2 %copy-start.1 = (f32[4,256,1024]{1,2,0:T(8,128)S(1)}, f32[4,256,1024]{1,2,0:T(8,128)}, u32[]{:S(2)}) copy-start(f32[4,256,1024]{1,2,0:T(8,128)} %get-tuple-element.245) | copy-start | bytes 12582916 | tf_op jit(solution)/shard_map/while
  103.4 1.8 %copy-start.5 = (f32[256,512]{1,0:T(8,128)S(1)}, f32[256,512]{1,0:T(8,128)}, u32[]{:S(2)}) copy-start(f32[256,512]{1,0:T(8,128)} %get-tuple-element.129) | copy-start | bytes 1572868
  103.4 1.8 %copy-start.8 = (f32[256]{0:T(256)S(1)}, f32[256]{0:T(256)}, u32[]{:S(2)}) copy-start(f32[256]{0:T(256)} %get-tuple-element.174) | copy-start | bytes 3076
  103.4 1.8 %copy-start.17 = (f32[512]{0:T(512)S(1)}, f32[512]{0:T(512)}, u32[]{:S(2)}) copy-start(f32[512]{0:T(512)} %param.35) | copy-start | bytes 6148
Sparse Core Ops, SparseCore 0:
  33.8 43.8 all-gather.1
  107.2 26.0 reduce-scatter.1
